TPU v7x, 32 devices: a whole 2x2x4 slice. The times are simulated.
32 devices in a mesh: fs: 16 (over z, y, x), tp: 2 (over core).
Axes of the slice: x: 2, y: 2, z: 4, core: 2. Of those that a mesh axis runs over, the one named last changes fastest.
Arguments:
- prompt: bfloat16 [5120, 2048], P('fs', 'tp'), may hold values from -6 to 6
- norm_gain: float32 [2048], P('fs'), may hold values from 0.1 to 1.9
- gate_master: float32 [2048, 3072], P('fs', 'tp'), may hold values from -0.125 to 0.125
- up_master: float32 [2048, 3072], P('fs', 'tp'), may hold values from -0.125 to 0.125
- down_master: float32 [2048, 3072], P('fs', 'tp'), may hold values from -0.109375 to 0.109375
Outputs:
- gate_new: bfloat16 [3072, 2048], P('tp')
- up_new: bfloat16 [3072, 2048], P('tp')
- down_new: bfloat16 [3072, 2048], P('tp')
- mixed: bfloat16 [2048, 5120], P('tp', 'fs')
All inputs are finite; a program needn't handle non-finite values.
Results may differ from a plain program's by a relative error of at most 0.0082.
Values may be sent and summed in bfloat16 or wider, within the bound.
A program may use at most 128 MiB of HBM per device.

v0:
```python
import jax
import jax.numpy as jnp
from jax import lax
from jax.sharding import PartitionSpec as P


def on_device(prompt, norm_gain, gate_master, up_master, down_master):
    gain_col = norm_gain[:, None]
    gate_low = (gate_master * gain_col).astype(jnp.bfloat16).T
    up_low = (up_master * gain_col).astype(jnp.bfloat16).T
    down_low = down_master.astype(jnp.bfloat16).T
    whole = lax.all_gather(prompt, "tp", axis=1, tiled=True)
    values = whole.astype(jnp.float32)
    normed = (values * lax.rsqrt(jnp.mean(values * values, axis=1, keepdims=True) + 1e-06)).astype(
        jnp.bfloat16
    )
    contract = (((1,), (1,)), ((), ()))
    gate_new, up_new, down_new = (
        lax.all_gather(gate_low, "fs", axis=1, tiled=True),
        lax.all_gather(up_low, "fs", axis=1, tiled=True),
        lax.all_gather(down_low, "fs", axis=1, tiled=True),
    )
    gate = lax.dot_general(normed, gate_new, contract, preferred_element_type=jnp.float32)
    up = lax.dot_general(normed, up_new, contract, preferred_element_type=jnp.float32)
    hidden = (jax.nn.silu(gate) * up).astype(jnp.bfloat16)
    mixed = lax.psum_scatter(
        lax.dot_general(
            down_new, hidden, (((0,), (1,)), ((), ())), preferred_element_type=jnp.float32
        ),
        "tp",
        scatter_dimension=0,
        tiled=True,
    )
    return (gate_new, up_new, down_new, mixed.astype(jnp.bfloat16))


def solution(mesh):
    placed = (P("fs", "tp"), P("fs"), P("fs", "tp"), P("fs", "tp"), P("fs", "tp"))
    return jax.shard_map(
        on_device,
        mesh=mesh,
        in_specs=placed,
        out_specs=(P("tp", None), P("tp", None), P("tp", None), P("tp", "fs")),
        check_vma=False,
    )
```

profile of v0, /device:TPU:0, one launch (start us, length us, event | category | flops | bytes accessed | tf_op | source)
XLA Modules:
  0.0 414.9 jit_solution(16847187545937609317)
XLA Ops:
  7.2 0.0 copy-start.1
  7.2 0.0 copy-start.3
  7.2 0.0 all-gather.11.cloned.1.call-start
  7.2 0.7 all-gather.11.cloned.1.call-update
  7.9 0.0 all-gather.5.cloned.1.call-start
  8.0 1.4 copy.10
  9.4 0.0 copy-done.1
  9.4 0.0 copy-start.2
  9.4 0.3 copy.9
  9.7 0.0 copy-done.3
  9.7 1.0 fusion.8
  10.7 0.0 all-gather.5.cloned.1.call-update
  10.7 0.0 all-gather.7.cloned.1.call-start
  10.7 0.7 all-gather.7.cloned.1.call-update
  11.4 0.0 all-gather.9.cloned.1.call-start
  11.5 0.0 copy-done.2
  11.5 0.9 copy.11
  12.4 0.0 all-gather.9.cloned.1.call-update
  12.4 0.0 reduce-scatter.2.cloned.1.call-start
  12.5 9.2 %all-gather.11.cloned.1.call-done = bf16[320,2048]{1,0:T(8,128)(2,1)} async-done(((bf16[320,1024]{1,0:T(8,128)(2,1)}), bf16[320,2048]{1,0:T(8,128)(2,1)}) %all-gather.11.cloned.1.call-update) | async-done | bytes 1310736 | tf_op jit(solution)/shard_map/all_gather | solution.py:12
  21.7 1.7 fusion.1
  23.4 0.0 copy-start
  23.4 117.8 %all-gather.5.cloned.1.call-done = bf16[1536,2048]{1,0:T(8,128)(2,1)} async-done(((bf16[1536,128]{1,0:T(8,128)(2,1)}), bf16[1536,2048]{1,0:T(8,128)(2,1)}) %all-gather.5.cloned.1.call-update) | async-done | bytes 6291472 | tf_op jit(solution)/shard_map/all_gather | solution.py:19
  141.2 5.4 %fusion.5 = f32[320,1536]{1,0:T(8,128)S(1)} fusion(bf16[1536,2048]{1,0:T(8,128)(2,1)} %all-gather.5.cloned.1.call-done, bf16[320,2048]{1,0:T(8,128)(2,1)} %all-gather.11.cloned.1.call-done, f32[320]{0:T(512)S(1)} %add_rsqrt_fusion), kind=kOutput, calls=%fused_computation.9 | convolution fusion | flops 2015232000 | bytes 9569536 | tf_op jit(solution)/shard_map/dot_general | solution.py:23
  146.6 111.1 %all-gather.7.cloned.1.call-done = bf16[1536,2048]{1,0:T(8,128)(2,1)} async-done(((bf16[1536,128]{1,0:T(8,128)(2,1)}), bf16[1536,2048]{1,0:T(8,128)(2,1)}) %all-gather.7.cloned.1.call-update) | async-done | bytes 6291472 | tf_op jit(solution)/shard_map/all_gather | solution.py:20
  257.7 116.4 %all-gather.9.cloned.1.call-done = bf16[1536,2048]{1,0:T(8,128)(2,1)} async-done(((bf16[1536,128]{1,0:T(8,128)(2,1)}), bf16[1536,2048]{1,0:T(8,128)(2,1)}) %all-gather.9.cloned.1.call-update) | async-done | bytes 6291472 | tf_op jit(solution)/shard_map/all_gather | solution.py:21
  374.1 0.0 copy-done
  374.1 10.6 %convolution_bitcast_fusion = f32[2048,320]{0,1:T(8,128)} fusion(bf16[1536,2048]{1,0:T(8,128)(2,1)} %all-gather.9.cloned.1.call-done, bf16[1536,2048]{1,0:T(8,128)(2,1)} %all-gather.7.cloned.1.call-done, f32[320,1536]{1,0:T(8,128)S(1)} %fusion.5, bf16[320,2048]{1,0:T(8,128)(2,1)S(1)} %copy-done, f32[320]{0:T(512)S(1)} %add_rsqrt_fusion), kind=kOutput, calls=%fused_computation.3 | convolution fusion | flops 4031447040 | bytes 18482432 | tf_op jit(solution)/shard_map/dot_general | solution.py:27
  384.7 0.0 reduce-scatter.2.cloned.1.call-update
  384.7 8.7 %reduce-scatter.2.cloned.1.call-done = f32[1024,320]{0,1:T(8,128)} async-done(((f32[2048,320]{0,1:T(8,128)}), f32[1024,320]{0,1:T(8,128)}) %reduce-scatter.2.cloned.1.call-update) | async-done | bytes 1310736 | tf_op jit(solution)/shard_map/reduce_scatter | solution.py:26
  393.4 0.0 slice-start
  393.4 2.4 convert_element_type.27
  395.8 0.0 slice-start.1
  395.8 0.0 slice-start.2
  395.8 6.8 %copy.15 = bf16[1536,2048]{1,0:T(8,128)(2,1)} copy(bf16[1536,2048]{1,0:T(8,128)(2,1)} %all-gather.5.cloned.1.call-done) | data formatting | bytes 12582912
  402.6 0.0 slice-done
  402.6 0.0 slice-done.1
  402.6 0.0 slice-start.3
  402.6 2.8 copy.16
  405.4 0.0 slice-done.2
  405.4 0.3 slice-done.3
  405.7 2.7 copy.17
  (3 shorter events, 0.0 us)
Async XLA Ops:
  7.2 2.2 copy-start.1
  7.2 2.5 copy-start.3
  7.2 14.5 %all-gather.11.cloned.1.call-start = ((), (), s32[]{:S(2)}) async-start(), calls=%async_computation.4 | async-start | bytes 1966080 | tf_op jit(solution)/shard_map/all_gather | solution.py:12
  7.9 133.3 %all-gather.5.cloned.1.call-start = ((), (), s32[]{:S(2)}) async-start(), calls=%async_computation.1 | async-start | bytes 6684672 | tf_op jit(solution)/shard_map/all_gather | solution.py:19
  9.4 2.1 copy-start.2
  10.7 247.0 %all-gather.7.cloned.1.call-start = ((), (), s32[]{:S(2)}) async-start(), calls=%async_computation.2 | async-start | bytes 6684672 | tf_op jit(solution)/shard_map/all_gather | solution.py:20
  11.4 362.7 %all-gather.9.cloned.1.call-start = ((), (), s32[]{:S(2)}) async-start(), calls=%async_computation.3 | async-start | bytes 6684672 | tf_op jit(solution)/shard_map/all_gather | solution.py:21
  12.4 381.0 %reduce-scatter.2.cloned.1.call-start = ((), (), s32[]{:S(2)}) async-start(), calls=%async_computation.5 | async-start | bytes 3932160 | tf_op jit(solution)/shard_map/reduce_scatter | solution.py:26
  23.4 350.7 %copy-start = (bf16[320,2048]{1,0:T(8,128)(2,1)S(1)}, bf16[320,2048]{1,0:T(8,128)(2,1)}, u32[]{:S(2)}) copy-start(bf16[320,2048]{1,0:T(8,128)(2,1)} %all-gather.11.cloned.1.call-done) | copy-start | bytes 3932164
  393.4 9.2 %slice-start = ((s8[6291456]{0:T(1024)(128)(4,1)}), s8[4194304]{0:T(1024)(128)(4,1)S(1)}, s32[]{:S(2)}) async-start(s8[6291456]{0:T(1024)(128)(4,1)} %bitcast.12), calls=%async_computation.6 | async-start | bytes 8388608
  395.8 6.8 %slice-start.1 = ((s8[6291456]{0:T(1024)(128)(4,1)}), s8[2097152]{0:T(1024)(128)(4,1)S(1)}, s32[]{:S(2)}) async-start(s8[6291456]{0:T(1024)(128)(4,1)} %bitcast.12), calls=%async_computation.7 | async-start | bytes 4194304
  395.8 9.6 %slice-start.2 = ((s8[6291456]{0:T(1024)(128)(4,1)}), s8[4194304]{0:T(1024)(128)(4,1)S(1)}, s32[]{:S(2)}) async-start(s8[6291456]{0:T(1024)(128)(4,1)} %bitcast.14), calls=%async_computation.8 | async-start | bytes 8388608
  402.6 3.1 slice-start.3
Sparse Core Ops, SparseCore 0:
  9.5 12.1 all-gather.10
  25.0 116.1 all-gather.4
  144.5 113.1 all-gather.6
  260.9 113.1 all-gather.8
  384.9 8.4 reduce-scatter.1
where the time goes:
time: 415 us
  waiting for transfers between devices  365 us (88%)
  matrix products  16 us (4%)
  local copies, waits for them, and re-layouts  15.2 us (4%)
  between operations  13.9 us (3%)
  other arithmetic  5.08 us (1%)
    all_gather x1, waiting for transfers between devices, on_device(): lax.all_gather(gate_low, 'fs', axis=1, tiled=True)  118 us
    all_gather x1, waiting for transfers between devices, on_device(): lax.all_gather(down_low, 'fs', axis=1, tiled=True)  116 us
    all_gather x1, waiting for transfers between devices, on_device(): lax.all_gather(up_low, 'fs', axis=1, tiled=True)  111 us
    unnamed x22, local copies, waits for them, and re-layouts  15.2 us
    dot_general x1, matrix products, on_device(): lax.dot_general(down_new, hidden, (((0,), (1,)), ((), ())), preferred_ele...  10.6 us
    all_gather x1, waiting for transfers between devices, on_device(): whole = lax.all_gather(prompt, 'tp', axis=1, tiled=True)  9.23 us
    reduce_scatter x1, waiting for transfers between devices, on_device(): lax.psum_scatter(lax.dot_general(down_new, hidden, (((0,), (1,)), ((), ()...  8.65 us
  transfers between devices with their start and end apart: 5, of which 5 were waited for; matrix products, arithmetic and copies ran while one was open for 3% of the time, Pallas kernels for 0%

commit v1 on v0

--- a/solution.py
+++ b/solution.py
@@ -16,7 +16,7 @@
     )
     contract = (((1,), (1,)), ((), ()))
     gate_new, up_new, down_new = (
-        lax.all_gather(gate_low, "fs", axis=1, tiled=True),
+        jnp.concatenate(lax.all_gather(gate_low, "fs"), axis=1),
         lax.all_gather(up_low, "fs", axis=1, tiled=True),
         lax.all_gather(down_low, "fs", axis=1, tiled=True),
     )

time: 415 us -> 391 us (0.942)
  waiting for transfers between devices: 365 us -> 339 us
  local copies, waits for them, and re-layouts: 15.2 us -> 19.4 us
    all_gather x1, waiting for transfers between devices: 118 us -> 96.3 us  [on_device(): lax.all_gather(gate_low, 'fs')]
    reshape x0 -> x1, local copies, waits for them, and re-layouts: none -> 4.69 us  [on_device(): jnp.concatenate(lax.all_gather(gate_low, 'fs'), axis=1)]
    unnamed x22 -> x19, local copies, waits for them, and re-layouts: 15.2 us -> 14.8 us
where the time goes in v1:
time: 391 us
  waiting for transfers between devices  339 us (87%)
  local copies, waits for them, and re-layouts  19.4 us (5%)
  between operations  13.9 us (4%)
  matrix products  12.9 us (3%)
  other arithmetic  5.08 us (1%)
    all_gather x1, waiting for transfers between devices, on_device(): lax.all_gather(down_low, 'fs', axis=1, tiled=True)  116 us
    all_gather x1, waiting for transfers between devices, on_device(): lax.all_gather(up_low, 'fs', axis=1, tiled=True)  107 us
    all_gather x1, waiting for transfers between devices, on_device(): lax.all_gather(gate_low, 'fs')  96.3 us
    unnamed x19, local copies, waits for them, and re-layouts  14.8 us
    dot_general x1, matrix products, on_device(): lax.dot_general(down_new, hidden, (((0,), (1,)), ((), ())), preferred_ele...  10.6 us
    all_gather x1, waiting for transfers between devices, on_device(): whole = lax.all_gather(prompt, 'tp', axis=1, tiled=True)  9.24 us
    reduce_scatter x1, waiting for transfers between devices, on_device(): lax.psum_scatter(lax.dot_general(down_new, hidden, (((0,), (1,)), ((), ()...  8.65 us
  transfers between devices with their start and end apart: 5, of which 5 were waited for; matrix products, arithmetic and copies ran while one was open for 3% of the time, Pallas kernels for 0%

profile of v1, /device:TPU:0, one launch (start us, length us, event | category | flops | bytes accessed | tf_op | source)
XLA Modules:
  0.0 390.6 jit_solution(14921053445615602)
XLA Ops:
  7.2 0.0 copy-start.2
  7.2 0.0 copy-start.4
  7.2 0.0 all-gather.10.cloned.1.call-start
  7.2 0.7 all-gather.10.cloned.1.call-update
  7.9 0.0 all-gather.12.cloned.1.call-start
  8.0 1.4 copy.11
  9.4 0.0 copy-done.2
  9.4 0.0 copy-start.3
  9.4 0.3 copy.9
  9.7 0.0 copy-done.4
  9.7 1.0 fusion.8
  10.7 0.0 all-gather.12.cloned.1.call-update
  10.7 0.0 all-gather.6.cloned.1.call-start
  10.7 0.7 all-gather.6.cloned.1.call-update
  11.4 0.0 all-gather.8.cloned.1.call-start
  11.5 0.0 copy-done.3
  11.5 0.9 copy.12
  12.4 0.0 all-gather.8.cloned.1.call-update
  12.4 0.0 reduce-scatter.2.cloned.1.call-start
  12.5 9.2 %all-gather.10.cloned.1.call-done = bf16[320,2048]{1,0:T(8,128)(2,1)} async-done(((bf16[320,1024]{1,0:T(8,128)(2,1)}), bf16[320,2048]{1,0:T(8,128)(2,1)}) %all-gather.10.cloned.1.call-update) | async-done | bytes 1310736 | tf_op jit(solution)/shard_map/all_gather | solution.py:12
  21.7 1.7 fusion.1
  23.4 96.3 %all-gather.12.cloned.1.call-done = bf16[24576,128]{1,0:T(8,128)(2,1)} async-done(((bf16[1536,128]{1,0:T(8,128)(2,1)}), bf16[24576,128]{1,0:T(8,128)(2,1)}) %all-gather.12.cloned.1.call-update) | async-done | bytes 6291472 | tf_op jit(solution)/shard_map/all_gather | solution.py:19
  119.7 0.0 copy-start.1
  119.7 4.7 %copy.15 = bf16[16,192,8,128]{3,2,0,1:T(8,128)(2,1)S(1)} copy(bf16[16,192,8,128]{3,2,1,0:T(8,128)(2,1)} %bitcast.21) | data formatting | bytes 12582912 | tf_op jit(solution)/shard_map/reshape | solution.py:19
  124.4 0.0 copy-start
  124.4 2.7 copy-done
  127.1 0.0 copy-done.1
  127.1 2.2 fusion.5
  129.3 107.2 %all-gather.6.cloned.1.call-done = bf16[1536,2048]{1,0:T(8,128)(2,1)} async-done(((bf16[1536,128]{1,0:T(8,128)(2,1)}), bf16[1536,2048]{1,0:T(8,128)(2,1)}) %all-gather.6.cloned.1.call-update) | async-done | bytes 6291472 | tf_op jit(solution)/shard_map/all_gather | solution.py:20
  236.5 116.4 %all-gather.8.cloned.1.call-done = bf16[1536,2048]{1,0:T(8,128)(2,1)} async-done(((bf16[1536,128]{1,0:T(8,128)(2,1)}), bf16[1536,2048]{1,0:T(8,128)(2,1)}) %all-gather.8.cloned.1.call-update) | async-done | bytes 6291472 | tf_op jit(solution)/shard_map/all_gather | solution.py:21
  352.9 10.6 %convolution_bitcast_fusion = f32[2048,320]{0,1:T(8,128)} fusion(bf16[1536,2048]{1,0:T(8,128)(2,1)} %all-gather.8.cloned.1.call-done, bf16[1536,2048]{1,0:T(8,128)(2,1)} %all-gather.6.cloned.1.call-done, f32[320,1536]{1,0:T(8,128)S(1)} %fusion.5, bf16[320,2048]{1,0:T(8,128)(2,1)S(1)} %copy-done.1, f32[320]{0:T(512)S(1)} %add_rsqrt_fusion), kind=kOutput, calls=%fused_computation.4 | convolution fusion | flops 4031447040 | bytes 18482432 | tf_op jit(solution)/shard_map/dot_general | solution.py:27
  363.5 0.0 reduce-scatter.2.cloned.1.call-update
  363.6 8.7 %reduce-scatter.2.cloned.1.call-done = f32[1024,320]{0,1:T(8,128)} async-done(((f32[2048,320]{0,1:T(8,128)}), f32[1024,320]{0,1:T(8,128)}) %reduce-scatter.2.cloned.1.call-update) | async-done | bytes 1310736 | tf_op jit(solution)/shard_map/reduce_scatter | solution.py:26
  372.2 0.0 slice-start
  372.2 2.4 convert_element_type.27
  374.6 0.0 slice-start.1
  374.6 6.8 %copy.18 = bf16[1536,2048]{1,0:T(8,128)(2,1)} copy(bf16[1536,2048]{1,0:T(8,128)(2,1)} %all-gather.6.cloned.1.call-done) | data formatting | bytes 12582912
  381.4 0.0 slice-done
  381.4 0.0 slice-done.1
  381.4 2.7 copy.19
  (2 shorter events, 0.0 us)
Async XLA Ops:
  7.2 2.2 copy-start.2
  7.2 2.5 copy-start.4
  7.2 14.5 %all-gather.10.cloned.1.call-start = ((), (), s32[]{:S(2)}) async-start(), calls=%async_computation.3 | async-start | bytes 1966080 | tf_op jit(solution)/shard_map/all_gather | solution.py:12
  7.9 111.7 %all-gather.12.cloned.1.call-start = ((), (), s32[]{:S(2)}) async-start(), calls=%async_computation.5 | async-start | bytes 6684672 | tf_op jit(solution)/shard_map/all_gather | solution.py:19
  9.4 2.1 copy-start.3
  10.7 225.9 %all-gather.6.cloned.1.call-start = ((), (), s32[]{:S(2)}) async-start(), calls=%async_computation.1 | async-start | bytes 6684672 | tf_op jit(solution)/shard_map/all_gather | solution.py:20
  11.4 341.5 %all-gather.8.cloned.1.call-start = ((), (), s32[]{:S(2)}) async-start(), calls=%async_computation.2 | async-start | bytes 6684672 | tf_op jit(solution)/shard_map/all_gather | solution.py:21
  12.4 359.8 %reduce-scatter.2.cloned.1.call-start = ((), (), s32[]{:S(2)}) async-start(), calls=%async_computation.4 | async-start | bytes 3932160 | tf_op jit(solution)/shard_map/reduce_scatter | solution.py:26
  119.7 7.4 %copy-start.1 = (bf16[320,2048]{1,0:T(8,128)(2,1)S(1)}, bf16[320,2048]{1,0:T(8,128)(2,1)}, u32[]{:S(2)}) copy-start(bf16[320,2048]{1,0:T(8,128)(2,1)} %all-gather.10.cloned.1.call-done) | copy-start | bytes 3932164
  124.4 2.7 copy-start
  372.2 9.2 %slice-start = ((s8[6291456]{0:T(1024)(128)(4,1)}), s8[4194304]{0:T(1024)(128)(4,1)S(1)}, s32[]{:S(2)}) async-start(s8[6291456]{0:T(1024)(128)(4,1)} %bitcast.19), calls=%async_computation.6 | async-start | bytes 8388608
  374.6 6.8 %slice-start.1 = ((s8[6291456]{0:T(1024)(128)(4,1)}), s8[2097152]{0:T(1024)(128)(4,1)S(1)}, s32[]{:S(2)}) async-start(s8[6291456]{0:T(1024)(128)(4,1)} %bitcast.19), calls=%async_computation.7 | async-start | bytes 4194304
Sparse Core Ops, SparseCore 0:
  9.5 12.1 all-gather.9
  25.1 94.5 all-gather.11
  122.9 113.5 all-gather.5
  239.7 113.1 all-gather.7
  363.7 8.4 reduce-scatter.1
